TPU v7x, 32 devices: a whole 2x2x4 slice. The times are simulated.
32 devices in a mesh: sp: 8 (over z, y), tp: 4 (over x, core).
Axes of the slice: x: 2, y: 2, z: 4, core: 2. Of those that a mesh axis runs over, the one named last changes fastest.
Arguments:
- tokens: bfloat16 [3072, 2048], P('sp', 'tp'), may hold values from -6 to 6
- norm_gain: float32 [2048], replicated, may hold values from 0.1 to 1.9
- w_query_down: bfloat16 [2048, 512], replicated, may hold values from -0.125 to 0.125
- query_gain: float32 [512], replicated, may hold values from 0.1 to 1.9
- w_query_up: bfloat16 [512, 1536], P(None, 'tp'), may hold values from -0.25 to 0.25
- w_latent_down: bfloat16 [2048, 256], replicated, may hold values from -0.125 to 0.125
- latent_gain: float32 [256], replicated, may hold values from 0.1 to 1.9
- w_rotary_key: bfloat16 [2048, 32], replicated, may hold values from -0.125 to 0.125
- w_latent_up: bfloat16 [256, 2048], P(None, 'tp'), may hold values from -0.375 to 0.375
- query_head_gain: float32 [96], replicated, may hold values from 0.1 to 1.9
- key_head_gain: float32 [96], replicated, may hold values from 0.1 to 1.9
- w_pool_in: bfloat16 [2048, 1024], P(None, 'tp'), may hold values from -0.125 to 0.125
- w_pool_mix: bfloat16 [4, 256, 256], P('tp'), may hold values from -0.375 to 0.375
- pool_scale: float32 [1024], P('tp'), may hold values from 0.1 to 1.9
- w_attn_out: bfloat16 [1024, 2048], P('tp'), may hold values from -12 to 12
- w_pool_out: bfloat16 [1024, 2048], P('tp'), may hold values from -0.5 to 0.5
- w_gate_attn: bfloat16 [2048, 2048], P(None, 'tp'), may hold values from -0.125 to 0.125
- w_gate_pool: bfloat16 [2048, 2048], P(None, 'tp'), may hold values from -0.125 to 0.125
Outputs:
- mixed: bfloat16 [3072, 2048], P('sp', 'tp')
All inputs are finite; a program needn't handle non-finite values.
Results may differ from a plain program's by a relative error of at most 0.02.
Values may be sent and summed in bfloat16 or wider, within the bound.
A program may use at most 128 MiB of HBM per device.

v0:
```python
import jax
import jax.numpy as jnp
from jax import lax
from jax.sharding import PartitionSpec as P

NOPE = 64
ROPE = 32
VALUE_DIM = 64
POOL_GROUPS = 4
POOL_GROUP = 256
eps = 1e-06
theta = 10000.0


def extended(cells, sides, width):
    for axis, dim in sides:
        count = lax.axis_size(axis)
        ends = count - 1
        head = lax.slice_in_dim(cells, 0, width, axis=dim)
        tail = lax.slice_in_dim(cells, cells.shape[dim] - width, cells.shape[dim], axis=dim)
        cells = jnp.concatenate(
            [
                lax.ppermute(tail, axis, [(i, (i + 1) % count) for i in range(ends)]),
                cells,
                lax.ppermute(head, axis, [((i + 1) % count, i) for i in range(ends)]),
            ],
            axis=dim,
        )
    return cells


def rms_scale(values, gain):
    values = values.astype(jnp.float32)
    return values * lax.rsqrt(jnp.mean(values * values, axis=-1, keepdims=True) + eps) * gain


def rotate(values, positions):
    half = values.shape[-1] // 2
    freqs = theta ** (-jnp.arange(half, dtype=jnp.float32) / half)
    angles = positions.astype(jnp.float32)[:, None] * freqs[None, :]
    cosine = jnp.cos(angles)[:, None, :]
    sine = jnp.sin(angles)[:, None, :]
    first = values[..., :half]
    second = values[..., half:]
    return jnp.concatenate(
        [first * cosine - second * sine, first * sine + second * cosine], axis=-1
    )


def head_finish(values, gain, positions):
    normed = rms_scale(values, gain)
    return jnp.concatenate([normed[..., :NOPE], rotate(normed[..., NOPE:], positions)], axis=-1)


def body(
    tokens,
    norm_gain,
    w_query_down,
    query_gain,
    w_query_up,
    w_latent_down,
    latent_gain,
    w_rotary_key,
    w_latent_up,
    query_head_gain,
    key_head_gain,
    w_pool_in,
    w_pool_mix,
    pool_scale,
    w_attn_out,
    w_pool_out,
    w_gate_attn,
    w_gate_pool,
):
    bf = jnp.bfloat16
    rows = tokens.shape[0]
    length = rows * lax.axis_size("sp")
    local_heads = w_query_up.shape[1] // (NOPE + ROPE)
    positions = lax.axis_index("sp") * rows + jnp.arange(rows, dtype=jnp.int32)
    whole = lax.all_gather(tokens, "tp", axis=1, tiled=True)
    normed = rms_scale(whole, norm_gain).astype(bf)
    query_latent = jnp.dot(normed, w_query_down, preferred_element_type=jnp.float32).astype(bf)
    query_normed = rms_scale(query_latent, query_gain).astype(bf)
    query_raw = jnp.dot(query_normed, w_query_up, preferred_element_type=jnp.float32).astype(bf)
    query_raw = query_raw.reshape(rows, local_heads, NOPE + ROPE)
    query = (head_finish(query_raw, query_head_gain, positions) * (NOPE + ROPE) ** (-0.5)).astype(
        bf
    )
    latent = jnp.dot(normed, w_latent_down, preferred_element_type=jnp.float32).astype(bf)
    key_latent = rms_scale(latent, latent_gain).astype(bf)
    rotary_key = jnp.dot(normed, w_rotary_key, preferred_element_type=jnp.float32).astype(bf)
    start_state = (
        jnp.full((local_heads, rows), -1e30, jnp.float32),
        jnp.zeros((local_heads, rows), jnp.float32),
        jnp.zeros((local_heads, rows, VALUE_DIM), jnp.float32),
    )
    latent_piece = lax.all_gather(key_latent, "sp", axis=0, tiled=True)
    rotary_piece = lax.all_gather(rotary_key, "sp", axis=0, tiled=True)
    blocks = latent_piece.shape[0] // rows
    latent_blocks = latent_piece.reshape(blocks, rows, latent_piece.shape[1])
    rotary_blocks = rotary_piece.reshape(blocks, rows, rotary_piece.shape[1])

    def one_block(state, items):
        latent_block, rotary_block, number = items
        top, total, summed = state
        key_positions = number * rows + jnp.arange(rows, dtype=jnp.int32)
        keys_values = jnp.dot(latent_block, w_latent_up, preferred_element_type=jnp.float32).astype(
            bf
        )
        keys_values = keys_values.reshape(rows, local_heads, NOPE + VALUE_DIM)
        key_raw = jnp.concatenate(
            [
                keys_values[..., :NOPE],
                jnp.broadcast_to(rotary_block[:, None, :], (rows, local_heads, ROPE)),
            ],
            axis=-1,
        )
        key = head_finish(key_raw, key_head_gain, key_positions).astype(bf)
        values = keys_values[..., NOPE:]
        scores = jnp.einsum("qhd,khd->hqk", query, key, preferred_element_type=jnp.float32)
        new_top = jnp.maximum(top, jnp.max(scores, axis=-1))
        factor = jnp.exp(top - new_top)
        expo = jnp.exp(scores - new_top[..., None])
        total = total * factor + jnp.sum(expo, axis=-1)
        summed = summed * factor[..., None] + jnp.einsum(
            "hqk,khv->hqv", expo.astype(bf), values, preferred_element_type=jnp.float32
        )
        return ((new_top, total, summed), None)

    state, _ = lax.scan(
        one_block, start_state, (latent_blocks, rotary_blocks, jnp.arange(blocks, dtype=jnp.int32))
    )
    top, total, summed = state
    attn_rows = jnp.transpose(summed / total[..., None], (1, 0, 2)).reshape(
        rows, local_heads * VALUE_DIM
    )
    attn_rows = attn_rows.astype(bf)
    pool_input = jnp.dot(normed, w_pool_in, preferred_element_type=jnp.float32).astype(bf)
    reach = 2**POOL_GROUPS // 2
    padded = extended(pool_input, (("sp", 0),), reach).astype(jnp.float32)
    local_groups = w_pool_mix.shape[0]
    group_ids = lax.axis_index("tp") * local_groups + jnp.arange(local_groups, dtype=jnp.int32)
    windows = jnp.power(2, group_ids + 1)
    channel_window = jnp.repeat(windows, POOL_GROUP)
    pooled = jnp.zeros((rows, local_groups * POOL_GROUP), jnp.float32)
    for shift in range(-reach, reach):
        inside = (shift >= -(channel_window // 2)) & (
            shift <= channel_window - channel_window // 2 - 1
        )
        pooled = pooled + jnp.where(
            inside[None, :], padded[reach + shift : reach + shift + rows], 0.0
        )
    low = jnp.clip(positions[:, None] - channel_window[None, :] // 2, 0, length)
    high = jnp.clip(
        positions[:, None] + channel_window[None, :] - channel_window[None, :] // 2, 0, length
    )
    count = (high - low).astype(jnp.float32)
    pool_mixed = (pooled / count - pool_input.astype(jnp.float32)).astype(bf)
    pool_mixed = pool_mixed.reshape(rows, local_groups, POOL_GROUP)
    grouped = jnp.einsum("lgc,gcd->lgd", pool_mixed, w_pool_mix, preferred_element_type=jnp.float32)
    pool_rows = (grouped.reshape(rows, local_groups * POOL_GROUP) * pool_scale).astype(bf)
    gate_attn = jax.nn.sigmoid(jnp.dot(normed, w_gate_attn, preferred_element_type=jnp.float32))
    gate_pool = jax.nn.sigmoid(jnp.dot(normed, w_gate_pool, preferred_element_type=jnp.float32))
    attn_tokens, pool_tokens = (
        lax.all_to_all(attn_rows, "tp", split_axis=0, concat_axis=1, tiled=True),
        lax.all_to_all(pool_rows, "tp", split_axis=0, concat_axis=1, tiled=True),
    )
    attn_weight, pool_weight = (
        lax.all_gather(w_attn_out, "tp", axis=0, tiled=True),
        lax.all_gather(w_pool_out, "tp", axis=0, tiled=True),
    )
    attn_here = jnp.dot(attn_tokens, attn_weight, preferred_element_type=jnp.float32)
    pool_here = jnp.dot(pool_tokens, pool_weight, preferred_element_type=jnp.float32)
    attn_branch, pool_branch = (
        lax.all_to_all(
            attn_here.astype(jnp.bfloat16), "tp", split_axis=1, concat_axis=0, tiled=True
        ).astype(attn_here.dtype),
        lax.all_to_all(
            pool_here.astype(jnp.bfloat16), "tp", split_axis=1, concat_axis=0, tiled=True
        ).astype(pool_here.dtype),
    )
    return (gate_attn * attn_branch + gate_pool * pool_branch).astype(bf)


def solution(mesh):
    placed = (
        P("sp", "tp"),
        P(),
        P(),
        P(),
        P(None, "tp"),
        P(),
        P(),
        P(),
        P(None, "tp"),
        P(),
        P(),
        P(None, "tp"),
        P("tp", None, None),
        P("tp"),
        P("tp", None),
        P("tp", None),
        P(None, "tp"),
        P(None, "tp"),
    )
    return jax.shard_map(body, mesh=mesh, in_specs=placed, out_specs=P("sp", "tp"), check_vma=False)
```

profile of v0, /device:TPU:0, one launch (start us, length us, event | category | flops | bytes accessed | tf_op | source)
XLA Modules:
  0.0 212.7 jit_solution(344831506499883668)
XLA Ops:
  7.3 24.0 %all-gather.5.cloned.1.call-done = bf16[384,2048]{1,0:T(8,128)(2,1)} async-done(((bf16[384,512]{1,0:T(8,128)(2,1)}), bf16[384,2048]{1,0:T(8,128)(2,1)}) %all-gather.5.cloned.1.call-update) | async-done | bytes 1572880 | tf_op jit(solution)/shard_map/all_gather | solution.py:80
  33.1 2.6 %multiply_reduce_fusion.1 = (f32[384]{0:T(512)S(1)}, f32[384,256]{0,1:T(8,128)S(1)}) fusion(bf16[2048,256]{1,0:T(8,128)(2,1)} %param.25, bf16[384,2048]{1,0:T(8,128)(2,1)} %all-gather.5.cloned.1.call-done, f32[2048]{0:T(1024)} %param.21, f32[384]{0:T(512)S(1)} %add_rsqrt_fusion.4), kind=kOutput, calls=%fused_computation.112 | convolution fusion | flops 406191744 | bytes 3025920 | tf_op jit(solution)/shard_map/dot_general | solution.py:89
  38.3 2.6 %multiply_reduce_fusion = (f32[384]{0:T(512)S(1)}, f32[384,512]{1,0:T(8,128)S(1)}) fusion(bf16[2048,512]{1,0:T(8,128)(2,1)S(1)} %copy-done, bf16[384,2048]{1,0:T(8,128)(2,1)} %all-gather.5.cloned.1.call-done, f32[2048]{0:T(1024)S(1)} %copy-done.15, f32[384]{0:T(512)S(1)} %add_rsqrt_fusion.4), kind=kOutput, calls=%fused_computation.65 | convolution fusion | flops 809238144 | bytes 4467712 | tf_op jit(solution)/shard_map/dot_general | solution.py:82
  44.5 4.5 %collective-permute-start = (bf16[8,256]{1,0:T(8,128)(2,1)S(1)}, bf16[8,256]{1,0:T(8,128)(2,1)S(1)}, u32[]{:S(2)}, u32[]{:S(2)}) collective-permute-start(bf16[8,256]{1,0:T(8,128)(2,1)S(1)} %get-tuple-element.153), channel_id=1, source_target_pairs={{0,4},{4,8},{8,12},{12,16},{16,20},{20,24},{24,28},{1,5},{5,9},{9,... | collective-permute-start | bytes 12296 | tf_op jit(solution)/shard_map/ppermute | solution.py:23
  50.5 31.9 %all_gather.17 = bf16[3072,32]{0,1:T(8,128)(2,1)S(1)} all-gather(bf16[384,32]{0,1:T(8,128)(2,1)S(1)} %convolution_convert_fusion.7), channel_id=1, replica_groups=mesh['sp'=8,'tp'=4] {'sp'}, dimensions={0}, use_global_device_ids=true | all-gather | bytes 221184 | tf_op jit(solution)/shard_map/all_gather | solution.py:98
  85.3 4.0 %all-to-all-start.2 = ((bf16[4,96,256]{2,1,0:T(8,128)(2,1)}), bf16[4,96,256]{2,1,0:T(8,128)(2,1)}, u32[]{:S(2)}, u32[]{:S(2)}) async-start(bf16[4,96,256]{2,1,0:T(8,128)(2,1)} %multiply_convert_fusion.2), calls=%async_computation.2 | async-start | bytes 393216 | tf_op jit(solution)/shard_map/all_to_all | solution.py:166
  89.4 2.7 %copy.46 = bf16[3072,256]{1,0:T(8,128)(2,1)} copy(bf16[3072,256]{0,1:T(8,128)(2,1)} %all-gather.7.cloned.1.call-done) | data formatting | bytes 3145728
  92.1 73.3 %while.15 = (s32[]{:T(128)}, f32[4,384]{1,0:T(4,128)S(1)}, f32[4,384]{1,0:T(4,128)S(1)}, f32[4,384,64]{1,2,0:T(8,128)S(1)}, bf16[8,384,256]{2,1,0:T(8,128)(2,1)}...) while((s32[]{:T(128)}, f32[4,384]{1,0:T(4,128)S(1)}, ...), condition=%wide.region_8.9_spmd.clone, body=%wide.region_4.8_spmd.clone.sunk | while | flops 295714592 | bytes 23564012 | solution.py:130
  98.2 2.1 %fusion.99 = f32[4,384]{1,0:T(4,128)S(1)} fusion(f32[4,384,384]{2,1,0:T(8,128)} %get-tuple-element.235, f32[4,384]{1,0:T(4,128)S(1)} %select_maximum_fusion.2), kind=kLoop, calls=%fused_computation.4.clone.1 | loop fusion | flops 1178112 | bytes 2371584 | tf_op jit(solution)/shard_map/while/body/eval_jaxpr/reduce_sum | solution.py:124
  105.3 2.0 bitcast_reduce_fusion.2
  107.3 2.1 %fusion.99 = f32[4,384]{1,0:T(4,128)S(1)} fusion(f32[4,384,384]{2,1,0:T(8,128)} %get-tuple-element.235, f32[4,384]{1,0:T(4,128)S(1)} %select_maximum_fusion.2), kind=kLoop, calls=%fused_computation.4.clone.1 | loop fusion | flops 1178112 | bytes 2371584 | tf_op jit(solution)/shard_map/while/body/eval_jaxpr/reduce_sum | solution.py:124
  114.3 2.0 bitcast_reduce_fusion.2
  116.3 2.1 %fusion.99 = f32[4,384]{1,0:T(4,128)S(1)} fusion(f32[4,384,384]{2,1,0:T(8,128)} %get-tuple-element.235, f32[4,384]{1,0:T(4,128)S(1)} %select_maximum_fusion.2), kind=kLoop, calls=%fused_computation.4.clone.1 | loop fusion | flops 1178112 | bytes 2371584 | tf_op jit(solution)/shard_map/while/body/eval_jaxpr/reduce_sum | solution.py:124
  123.4 2.0 bitcast_reduce_fusion.2
  125.4 2.3 %fusion.99 = f32[4,384]{1,0:T(4,128)S(1)} fusion(f32[4,384,384]{2,1,0:T(8,128)} %get-tuple-element.235, f32[4,384]{1,0:T(4,128)S(1)} %select_maximum_fusion.2), kind=kLoop, calls=%fused_computation.4.clone.1 | loop fusion | flops 1178112 | bytes 2371584 | tf_op jit(solution)/shard_map/while/body/eval_jaxpr/reduce_sum | solution.py:124
  133.2 2.0 bitcast_reduce_fusion.2
  135.2 2.1 %fusion.99 = f32[4,384]{1,0:T(4,128)S(1)} fusion(f32[4,384,384]{2,1,0:T(8,128)} %get-tuple-element.235, f32[4,384]{1,0:T(4,128)S(1)} %select_maximum_fusion.2), kind=kLoop, calls=%fused_computation.4.clone.1 | loop fusion | flops 1178112 | bytes 2371584 | tf_op jit(solution)/shard_map/while/body/eval_jaxpr/reduce_sum | solution.py:124
  142.3 2.0 bitcast_reduce_fusion.2
  144.3 2.1 %fusion.99 = f32[4,384]{1,0:T(4,128)S(1)} fusion(f32[4,384,384]{2,1,0:T(8,128)} %get-tuple-element.235, f32[4,384]{1,0:T(4,128)S(1)} %select_maximum_fusion.2), kind=kLoop, calls=%fused_computation.4.clone.1 | loop fusion | flops 1178112 | bytes 2371584 | tf_op jit(solution)/shard_map/while/body/eval_jaxpr/reduce_sum | solution.py:124
  151.4 2.0 bitcast_reduce_fusion.2
  153.4 2.1 %fusion.99 = f32[4,384]{1,0:T(4,128)S(1)} fusion(f32[4,384,384]{2,1,0:T(8,128)} %get-tuple-element.235, f32[4,384]{1,0:T(4,128)S(1)} %select_maximum_fusion.2), kind=kLoop, calls=%fused_computation.4.clone.1 | loop fusion | flops 1178112 | bytes 2371584 | tf_op jit(solution)/shard_map/while/body/eval_jaxpr/reduce_sum | solution.py:124
  160.4 2.0 bitcast_reduce_fusion.2
  162.4 2.1 %fusion.99 = f32[4,384]{1,0:T(4,128)S(1)} fusion(f32[4,384,384]{2,1,0:T(8,128)} %get-tuple-element.235, f32[4,384]{1,0:T(4,128)S(1)} %select_maximum_fusion.2), kind=kLoop, calls=%fused_computation.4.clone.1 | loop fusion | flops 1178112 | bytes 2371584 | tf_op jit(solution)/shard_map/while/body/eval_jaxpr/reduce_sum | solution.py:124
  166.4 3.4 %all-to-all-start = ((bf16[4,96,256]{2,1,0:T(8,128)(2,1)}), bf16[4,96,256]{2,1,0:T(8,128)(2,1)S(1)}, u32[]{:S(2)}, u32[]{:S(2)}) async-start(bf16[4,96,256]{2,1,0:T(8,128)(2,1)} %copy.40), calls=%async_computation | async-start | bytes 393216 | tf_op jit(solution)/shard_map/all_to_all | solution.py:165
  170.8 4.4 %all-to-all-done = bf16[4,96,256]{2,1,0:T(8,128)(2,1)S(1)} async-done(((bf16[4,96,256]{2,1,0:T(8,128)(2,1)}), bf16[4,96,256]{2,1,0:T(8,128)(2,1)S(1)}, u32[]{:S(2)}, u32[]{:S(2)}) %all-to-all-start) | async-done | bytes 196640 | tf_op jit(solution)/shard_map/all_to_all | solution.py:165
  175.2 3.0 %convolution_convert_fusion.2 = bf16[96,2048]{1,0:T(8,128)(2,1)S(1)} fusion(bf16[96,1024]{1,0:T(8,128)(2,1)S(1)} %bitcast.121, bf16[1024,2048]{1,0:T(8,128)(2,1)} %all-gather.9.cloned.1.call-done), kind=kOutput, calls=%fused_computation.44 | convolution fusion | flops 402849792 | bytes 4784128 | tf_op jit(solution)/shard_map/dot_general | solution.py:172
  179.0 3.5 %all-to-all-start.1 = ((bf16[96,4,512]{2,0,1:T(8,128)(2,1)}), bf16[96,4,512]{2,0,1:T(8,128)(2,1)S(1)}, u32[]{:S(2)}, u32[]{:S(2)}) async-start(bf16[96,4,512]{2,0,1:T(8,128)(2,1)} %bitcast.93), calls=%async_computation.1 | async-start | bytes 786432 | tf_op jit(solution)/shard_map/all_to_all | solution.py:175
  182.5 3.0 %convolution_convert_fusion.1 = bf16[96,2048]{1,0:T(8,128)(2,1)S(1)} fusion(bf16[96,1024]{1,0:T(8,128)(2,1)S(1)} %bitcast.120, bf16[1024,2048]{1,0:T(8,128)(2,1)} %all-gather.11.cloned.1.call-done), kind=kOutput, calls=%fused_computation.43 | convolution fusion | flops 402849792 | bytes 4784128 | tf_op jit(solution)/shard_map/dot_general | solution.py:173
  186.3 3.6 %all-to-all-done.1 = bf16[96,4,512]{2,0,1:T(8,128)(2,1)S(1)} async-done(((bf16[96,4,512]{2,0,1:T(8,128)(2,1)}), bf16[96,4,512]{2,0,1:T(8,128)(2,1)S(1)}, u32[]{:S(2)}, u32[]{:S(2)}) %all-to-all-start.1) | async-done | bytes 393248 | tf_op jit(solution)/shard_map/all_to_all | solution.py:175
  189.8 3.5 %all-to-all-start.3 = ((bf16[96,4,512]{2,0,1:T(8,128)(2,1)}), bf16[96,4,512]{2,0,1:T(8,128)(2,1)S(1)}, u32[]{:S(2)}, u32[]{:S(2)}) async-start(bf16[96,4,512]{2,0,1:T(8,128)(2,1)} %bitcast.92), calls=%async_computation.3 | async-start | bytes 786432 | tf_op jit(solution)/shard_map/all_to_all | solution.py:178
  194.3 6.4 %all-to-all-done.3 = bf16[96,4,512]{2,0,1:T(8,128)(2,1)S(1)} async-done(((bf16[96,4,512]{2,0,1:T(8,128)(2,1)}), bf16[96,4,512]{2,0,1:T(8,128)(2,1)S(1)}, u32[]{:S(2)}, u32[]{:S(2)}) %all-to-all-start.3) | async-done | bytes 393248 | tf_op jit(solution)/shard_map/all_to_all | solution.py:178
  200.8 3.5 %fusion.26 = f32[384,512]{1,0:T(8,128)S(1)} fusion(f32[384,512]{1,0:T(8,128)} %bitcast.122, bf16[2048,512]{1,0:T(8,128)(2,1)} %param.36, bf16[384,2048]{1,0:T(8,128)(2,1)} %all-gather.5.cloned.1.call-done, f32[2048]{0:T(1024)S(1)} %copy-done.15, f32[384]{0:T(512)S(1)} %add_rsqrt_fusion.4), kind=kOutput, calls=%fused_computation.51 | convolution fusion | flops 809238528 | bytes 5252608 | tf_op jit(solution)/shard_map/dot_general | solution.py:162
  (257 shorter events, 55.1 us)
Async XLA Ops:
  6.5 31.7 %copy-start = (bf16[2048,512]{1,0:T(8,128)(2,1)S(1)}, bf16[2048,512]{1,0:T(8,128)(2,1)}, u32[]{:S(2)}) copy-start(bf16[2048,512]{1,0:T(8,128)(2,1)} %param.22) | copy-start | bytes 6291460
  6.5 24.7 %all-gather.5.cloned.1.call-start = ((), (), s32[]{:S(2)}) async-start(), calls=%async_computation.4 | async-start | bytes 1966080 | tf_op jit(solution)/shard_map/all_gather | solution.py:80
  7.3 82.1 %all-gather.7.cloned.1.call-start = ((), (), s32[]{:S(2)}) async-start(), calls=%async_computation.5 | async-start | bytes 1769472 | tf_op jit(solution)/shard_map/all_gather | solution.py:97
  33.1 2.6 %copy-start.8 = (f32[256]{0:T(256)S(1)}, f32[256]{0:T(256)}, u32[]{:S(2)}) copy-start(f32[256]{0:T(256)} %param.26) | copy-start | bytes 3076
  35.7 2.6 %copy-start.15 = (f32[2048]{0:T(1024)S(1)}, f32[2048]{0:T(1024)}, u32[]{:S(2)}) copy-start(f32[2048]{0:T(1024)} %param.21) | copy-start | bytes 24580
  36.5 138.7 %all-gather.9.cloned.1.call-start = ((), (), s32[]{:S(2)}) async-start(), calls=%async_computation.6 | async-start | bytes 5242880 | tf_op jit(solution)/shard_map/all_gather | solution.py:169
  37.3 145.2 %all-gather.11.cloned.1.call-start = ((), (), s32[]{:S(2)}) async-start(), calls=%async_computation.7 | async-start | bytes 5242880 | tf_op jit(solution)/shard_map/all_gather | solution.py:170
  38.3 2.6 %copy-start.5 = (bf16[512,384]{1,0:T(8,128)(2,1)S(1)}, bf16[512,384]{1,0:T(8,128)(2,1)}, u32[]{:S(2)}) copy-start(bf16[512,384]{1,0:T(8,128)(2,1)} %param.24) | copy-start | bytes 1179652
  38.3 2.6 %copy-start.7 = (f32[512]{0:T(512)S(1)}, f32[512]{0:T(512)}, u32[]{:S(2)}) copy-start(f32[512]{0:T(512)} %param.23) | copy-start | bytes 6148
  38.3 3.2 %copy-start.10 = (f32[96]{0:T(128)S(1)}, f32[96]{0:T(128)}, u32[]{:S(2)}) copy-start(f32[96]{0:T(128)} %param.29) | copy-start | bytes 1156
  42.6 7.3 %copy-start.13 = (bf16[2048,32]{0,1:T(8,128)(2,1)S(1)}, bf16[2048,32]{0,1:T(8,128)(2,1)}, u32[]{:S(2)}) copy-start(bf16[2048,32]{0,1:T(8,128)(2,1)} %param.27) | copy-start | bytes 393220
  43.2 39.9 %collective-permute-start.1 = (bf16[8,256]{1,0:T(8,128)(2,1)S(1)}, bf16[8,256]{1,0:T(8,128)(2,1)S(1)}, u32[]{:S(2)}, u32[]{:S(2)}) collective-permute-start(bf16[8,256]{1,0:T(8,128)(2,1)S(1)} %get-tuple-element.154), channel_id=1, source_target_pairs={{4,0},{8,4},{12,8},{16,12},{20,16},{24,20},{28,24},{5,1},{9,5},{13... | collective-permute-start | bytes 12296 | tf_op jit(solution)/shard_map/ppermute | solution.py:25
  44.5 38.6 %collective-permute-start = (bf16[8,256]{1,0:T(8,128)(2,1)S(1)}, bf16[8,256]{1,0:T(8,128)(2,1)S(1)}, u32[]{:S(2)}, u32[]{:S(2)}) collective-permute-start(bf16[8,256]{1,0:T(8,128)(2,1)S(1)} %get-tuple-element.153), channel_id=1, source_target_pairs={{0,4},{4,8},{8,12},{12,16},{16,20},{20,24},{24,28},{1,5},{5,9},{9,... | collective-permute-start | bytes 12296 | tf_op jit(solution)/shard_map/ppermute | solution.py:23
  49.1 34.1 %copy-start.14 = (bf16[1,256,256]{2,1,0:T(8,128)(2,1)S(1)}, bf16[1,256,256]{2,1,0:T(8,128)(2,1)}, u32[]{:S(2)}) copy-start(bf16[1,256,256]{2,1,0:T(8,128)(2,1)} %param.32) | copy-start | bytes 393220
  84.6 7.4 %copy-start.6 = (f32[96]{0:T(128)S(1)}, f32[96]{0:T(128)}, u32[]{:S(2)}) copy-start(f32[96]{0:T(128)} %param.30) | copy-start | bytes 1156
  85.3 81.1 %all-to-all-start.2 = ((bf16[4,96,256]{2,1,0:T(8,128)(2,1)}), bf16[4,96,256]{2,1,0:T(8,128)(2,1)}, u32[]{:S(2)}, u32[]{:S(2)}) async-start(bf16[4,96,256]{2,1,0:T(8,128)(2,1)} %multiply_convert_fusion.2), calls=%async_computation.2 | async-start | bytes 393216 | tf_op jit(solution)/shard_map/all_to_all | solution.py:166
  98.2 2.4 %copy-start.1 = (f32[4,384,384]{2,1,0:T(8,128)S(1)}, f32[4,384,384]{2,1,0:T(8,128)}, u32[]{:S(2)}) copy-start(f32[4,384,384]{2,1,0:T(8,128)} %get-tuple-element.235) | copy-start | bytes 7077892 | tf_op jit(solution)/shard_map/while
  107.3 2.4 %copy-start.1 = (f32[4,384,384]{2,1,0:T(8,128)S(1)}, f32[4,384,384]{2,1,0:T(8,128)}, u32[]{:S(2)}) copy-start(f32[4,384,384]{2,1,0:T(8,128)} %get-tuple-element.235) | copy-start | bytes 7077892 | tf_op jit(solution)/shard_map/while
  112.5 1.8 copy-start.2
  116.3 2.4 %copy-start.1 = (f32[4,384,384]{2,1,0:T(8,128)S(1)}, f32[4,384,384]{2,1,0:T(8,128)}, u32[]{:S(2)}) copy-start(f32[4,384,384]{2,1,0:T(8,128)} %get-tuple-element.235) | copy-start | bytes 7077892 | tf_op jit(solution)/shard_map/while
  125.4 3.1 %copy-start.1 = (f32[4,384,384]{2,1,0:T(8,128)S(1)}, f32[4,384,384]{2,1,0:T(8,128)}, u32[]{:S(2)}) copy-start(f32[4,384,384]{2,1,0:T(8,128)} %get-tuple-element.235) | copy-start | bytes 7077892 | tf_op jit(solution)/shard_map/while
  135.2 2.4 %copy-start.1 = (f32[4,384,384]{2,1,0:T(8,128)S(1)}, f32[4,384,384]{2,1,0:T(8,128)}, u32[]{:S(2)}) copy-start(f32[4,384,384]{2,1,0:T(8,128)} %get-tuple-element.235) | copy-start | bytes 7077892 | tf_op jit(solution)/shard_map/while
  140.5 1.8 copy-start.2
  144.3 2.4 %copy-start.1 = (f32[4,384,384]{2,1,0:T(8,128)S(1)}, f32[4,384,384]{2,1,0:T(8,128)}, u32[]{:S(2)}) copy-start(f32[4,384,384]{2,1,0:T(8,128)} %get-tuple-element.235) | copy-start | bytes 7077892 | tf_op jit(solution)/shard_map/while
  153.4 2.4 %copy-start.1 = (f32[4,384,384]{2,1,0:T(8,128)S(1)}, f32[4,384,384]{2,1,0:T(8,128)}, u32[]{:S(2)}) copy-start(f32[4,384,384]{2,1,0:T(8,128)} %get-tuple-element.235) | copy-start | bytes 7077892 | tf_op jit(solution)/shard_map/while
  158.6 1.8 copy-start.2
  162.4 2.4 %copy-start.1 = (f32[4,384,384]{2,1,0:T(8,128)S(1)}, f32[4,384,384]{2,1,0:T(8,128)}, u32[]{:S(2)}) copy-start(f32[4,384,384]{2,1,0:T(8,128)} %get-tuple-element.235) | copy-start | bytes 7077892 | tf_op jit(solution)/shard_map/while
  166.4 8.7 %all-to-all-start = ((bf16[4,96,256]{2,1,0:T(8,128)(2,1)}), bf16[4,96,256]{2,1,0:T(8,128)(2,1)S(1)}, u32[]{:S(2)}, u32[]{:S(2)}) async-start(bf16[4,96,256]{2,1,0:T(8,128)(2,1)} %copy.40), calls=%async_computation | async-start | bytes 393216 | tf_op jit(solution)/shard_map/all_to_all | solution.py:165
  179.0 10.8 %all-to-all-start.1 = ((bf16[96,4,512]{2,0,1:T(8,128)(2,1)}), bf16[96,4,512]{2,0,1:T(8,128)(2,1)S(1)}, u32[]{:S(2)}, u32[]{:S(2)}) async-start(bf16[96,4,512]{2,0,1:T(8,128)(2,1)} %bitcast.93), calls=%async_computation.1 | async-start | bytes 786432 | tf_op jit(solution)/shard_map/all_to_all | solution.py:175
  189.8 10.8 %all-to-all-start.3 = ((bf16[96,4,512]{2,0,1:T(8,128)(2,1)}), bf16[96,4,512]{2,0,1:T(8,128)(2,1)S(1)}, u32[]{:S(2)}, u32[]{:S(2)}) async-start(bf16[96,4,512]{2,0,1:T(8,128)(2,1)} %bitcast.92), calls=%async_computation.3 | async-start | bytes 786432 | tf_op jit(solution)/shard_map/all_to_all | solution.py:178
  200.7 3.6 %copy-start.4 = (bf16[384,2048]{1,0:T(8,128)(2,1)S(1)}, bf16[384,2048]{1,0:T(8,128)(2,1)}, u32[]{:S(2)}) copy-start(bf16[384,2048]{1,0:T(8,128)(2,1)} %all-gather.5.cloned.1.call-done) | copy-start | bytes 4718596
  200.8 3.6 %copy-start.11 = (bf16[2048,512]{1,0:T(8,128)(2,1)S(1)}, bf16[2048,512]{1,0:T(8,128)(2,1)}, u32[]{:S(2)}) copy-start(bf16[2048,512]{1,0:T(8,128)(2,1)} %param.37) | copy-start | bytes 6291460
  (8 other events, 13.6 us)
Sparse Core Ops, SparseCore 0:
  8.9 22.3 all-gather.4
  36.6 45.9 all-gather.6
  84.2 34.4 all-gather.8
  120.1 32.7 all-gather.10
where the time goes:
time: 214 us; the launch traced here: 213 us
  matrix products  50.5 us (24%)
  waiting for transfers between devices  40.3 us (19%)
  blocking collectives  31.9 us (15%)
  other arithmetic  26.5 us (12%)
  local copies, waits for them, and re-layouts  23.5 us (11%)
  starting transfers between devices  20.3 us (9%)
  between operations  13.7 us (6%)
  loops' own time  6.1 us (3%)
    all_gather x1, blocking collectives, body(): rotary_piece = lax.all_gather(rotary_key, 'sp', axis=0, tiled=True)  31.9 us
    all_gather x1, waiting for transfers between devices, body(): whole = lax.all_gather(tokens, 'tp', axis=1, tiled=True)  24 us
    reduce_sum x8, other arithmetic, one_block(): total = total * factor + jnp.sum(expo, axis=-1)  17.4 us
    dot_general x8, matrix products, one_block(): jnp.einsum('qhd,khd->hqk', query, key, preferred_element_type=jnp.float32)  16 us
    dot_general x8, matrix products, one_block(): jnp.dot(latent_block, w_latent_up, preferred_element_type=jnp.float32)  10.5 us
    all_to_all x1, waiting for transfers between devices, body(): lax.all_to_all(pool_here.astype(jnp.bfloat16), 'tp', split_axis=1, concat...  6.4 us
    another operation x1, loops' own time, body(): lax.scan(one_block, start_state, (latent_blocks, rotary_blocks, jnp.arang...  6.1 us
    broadcast_in_dim x16, local copies, waits for them, and re-layouts, one_block(): jnp.broadcast_to(rotary_block[:, None, :], (rows, local_heads, ROPE))  6.05 us
  transfers between devices with their start and end apart: 10, of which 4 were waited for; matrix products, arithmetic and copies ran while one was open for 41% of the time, Pallas kernels for 0%

commit v1 on v0

--- a/solution.py
+++ b/solution.py
@@ -77,7 +77,7 @@
     length = rows * lax.axis_size("sp")
     local_heads = w_query_up.shape[1] // (NOPE + ROPE)
     positions = lax.axis_index("sp") * rows + jnp.arange(rows, dtype=jnp.int32)
-    whole = lax.all_gather(tokens, "tp", axis=1, tiled=True)
+    whole = jnp.concatenate(lax.all_gather(tokens, "tp"), axis=1)
     normed = rms_scale(whole, norm_gain).astype(bf)
     query_latent = jnp.dot(normed, w_query_down, preferred_element_type=jnp.float32).astype(bf)
     query_normed = rms_scale(query_latent, query_gain).astype(bf)

time: 214 us -> 229 us (1.070)
  other arithmetic: 26.5 us -> 37.1 us
  local copies, waits for them, and re-layouts: 23.5 us -> 31.8 us
  waiting for transfers between devices: 40.3 us -> 37 us
    convert_element_type x0 -> x2, other arithmetic: none -> 5.94 us  [the longest x1 3.59 us: rms_scale(): values = values.astype(jnp.float32)]
    mul x9, other arithmetic: 0.98 us -> 6.25 us  [rms_scale(): values * lax.rsqrt(jnp.mean(values * values, axis=-1, keepdims=True) + eps)]
    dynamic_slice x8, local copies, waits for them, and re-layouts: 5.25 us -> 9.91 us  [body(): lax.scan(one_block, start_state, (latent_blocks, rotary_blocks, jnp.arang...]
    convert_element_type x0 -> x1, local copies, waits for them, and re-layouts: none -> 3.58 us  [rms_scale(): values = values.astype(jnp.float32)]
    all_to_all x1, waiting for transfers between devices: 6.4 us -> 3.18 us  [body(): lax.all_to_all(pool_here.astype(jnp.bfloat16), 'tp', split_axis=1, concat...]
  transfers between devices with their start and end apart: 10 -> 10, of which waited for: 4 -> 4; matrix products, arithmetic and copies ran while one was open for 41% -> 44% of each run, Pallas kernels for 0% -> 0%
where the time goes in v1:
time: 229 us; the launch traced here: 228 us
  matrix products  49.9 us (22%)
  other arithmetic  37.1 us (16%)
  waiting for transfers between devices  37 us (16%)
  blocking collectives  33.5 us (15%)
  local copies, waits for them, and re-layouts  31.8 us (14%)
  starting transfers between devices  19.2 us (8%)
  between operations  13.7 us (6%)
  loops' own time  5.65 us (2%)
    all_gather x1, blocking collectives, body(): rotary_piece = lax.all_gather(rotary_key, 'sp', axis=0, tiled=True)  33.5 us
    all_gather x1, waiting for transfers between devices, body(): whole = jnp.concatenate(lax.all_gather(tokens, 'tp'), axis=1)  24 us
    reduce_sum x8, other arithmetic, one_block(): total = total * factor + jnp.sum(expo, axis=-1)  17.1 us
    dot_general x8, matrix products, one_block(): jnp.einsum('qhd,khd->hqk', query, key, preferred_element_type=jnp.float32)  15.8 us
    dynamic_slice x8, local copies, waits for them, and re-layouts, body(): lax.scan(one_block, start_state, (latent_blocks, rotary_blocks, jnp.arang...  9.91 us
    dot_general x8, matrix products, one_block(): jnp.dot(latent_block, w_latent_up, preferred_element_type=jnp.float32)  9.5 us
    broadcast_in_dim x16, local copies, waits for them, and re-layouts, one_block(): jnp.broadcast_to(rotary_block[:, None, :], (rows, local_heads, ROPE))  6.38 us
    mul x9, other arithmetic, rms_scale(): values * lax.rsqrt(jnp.mean(values * values, axis=-1, keepdims=True) + eps)  6.25 us
  transfers between devices with their start and end apart: 10, of which 4 were waited for; matrix products, arithmetic and copies ran while one was open for 44% of the time, Pallas kernels for 0%

profile of v1, /device:TPU:0, one launch (start us, length us, event | category | flops | bytes accessed | tf_op | source)
XLA Modules:
  0.0 227.9 jit_solution(17712845649548550093)
XLA Ops:
  7.3 24.0 %all-gather.12.cloned.1.call-done = bf16[1536,512]{1,0:T(8,128)(2,1)} async-done(((bf16[384,512]{1,0:T(8,128)(2,1)}), bf16[1536,512]{1,0:T(8,128)(2,1)}) %all-gather.12.cloned.1.call-update) | async-done | bytes 1572880 | tf_op jit(solution)/shard_map/all_gather | solution.py:80
  31.3 3.6 %convert_bitcast_fusion = f32[384,4,512]{2,0,1:T(8,128)} fusion(bf16[4,384,512]{2,1,0:T(8,128)(2,1)} %bitcast.131), kind=kLoop, calls=%fused_computation.39 | loop fusion | flops 786432 | bytes 4718592 | tf_op jit(solution)/shard_map/convert_element_type | solution.py:33
  35.3 3.6 %copy.48 = f32[384,4,512]{0,2,1:T(8,128)} copy(f32[384,4,512]{2,0,1:T(8,128)} %convert_bitcast_fusion) | data formatting | bytes 6291456 | tf_op jit(solution)/shard_map/convert_element_type | solution.py:33
  38.9 2.3 %fusion.21 = bf16[384,2048]{0,1:T(8,128)(2,1)S(1)} fusion(f32[384,4,512]{0,2,1:T(8,128)} %copy.48, f32[2048]{0:T(1024)S(1)} %copy-done.12, f32[384]{0:T(512)S(1)} %add_rsqrt_fusion.4), kind=kLoop, calls=%fused_computation.43 | loop fusion | flops 2359296 | bytes 4728320 | tf_op jit(solution)/shard_map/convert_element_type | solution.py:81
  46.2 2.0 convolution_convert_fusion.5
  48.3 3.4 %collective-permute-start = (bf16[8,256]{1,0:T(8,128)(2,1)S(1)}, bf16[8,256]{1,0:T(8,128)(2,1)S(1)}, u32[]{:S(2)}, u32[]{:S(2)}) collective-permute-start(bf16[8,256]{1,0:T(8,128)(2,1)S(1)} %get-tuple-element.163), channel_id=1, source_target_pairs={{0,4},{4,8},{8,12},{12,16},{16,20},{20,24},{24,28},{1,5},{5,9},{9,... | collective-permute-start | bytes 12296 | tf_op jit(solution)/shard_map/ppermute | solution.py:23
  56.3 33.5 %all_gather.21 = bf16[3072,32]{0,1:T(8,128)(2,1)S(1)} all-gather(bf16[384,32]{0,1:T(8,128)(2,1)S(1)} %convolution_convert_fusion.7), channel_id=1, replica_groups=mesh['sp'=8,'tp'=4] {'sp'}, dimensions={0}, use_global_device_ids=true | all-gather | bytes 221184 | tf_op jit(solution)/shard_map/all_gather | solution.py:98
  92.7 4.0 %all-to-all-start.2 = ((bf16[4,96,256]{2,1,0:T(8,128)(2,1)}), bf16[4,96,256]{2,1,0:T(8,128)(2,1)}, u32[]{:S(2)}, u32[]{:S(2)}) async-start(bf16[4,96,256]{2,1,0:T(8,128)(2,1)} %multiply_convert_fusion.2), calls=%async_computation.2 | async-start | bytes 393216 | tf_op jit(solution)/shard_map/all_to_all | solution.py:166
  96.7 2.7 %copy.57 = bf16[3072,256]{1,0:T(8,128)(2,1)} copy(bf16[3072,256]{0,1:T(8,128)(2,1)} %all-gather.6.cloned.1.call-done) | data formatting | bytes 3145728
  100.0 81.2 %while.15 = (s32[]{:T(128)}, f32[4,384]{1,0:T(4,128)S(1)}, f32[4,384]{1,0:T(4,128)}, f32[4,384,64]{1,2,0:T(8,128)S(1)}, bf16[8,384,256]{2,1,0:T(8,128)(2,1)}, /*...) while((s32[]{:T(128)}, f32[4,384]{1,0:T(4,128)S(1)}, ...), condition=%wide.region_8.9_spmd.clone, body=%wide.region_4.8_spmd.clone.sunk | while | flops 295714592 | bytes 23613720 | solution.py:130
  105.2 2.0 bitcast_reduce_fusion.2
  107.2 2.1 fusion.99
  115.4 2.0 bitcast_reduce_fusion.2
  117.4 2.1 fusion.99
  127.5 2.1 fusion.99
  137.7 2.1 fusion.99
  145.9 2.0 bitcast_reduce_fusion.2
  147.8 2.1 fusion.99
  158.0 2.1 fusion.99
  168.2 2.1 fusion.99
  176.3 2.0 bitcast_reduce_fusion.2
  178.3 2.1 fusion.99
  183.0 3.4 %all-to-all-start = ((bf16[4,96,256]{2,1,0:T(8,128)(2,1)}), bf16[4,96,256]{2,1,0:T(8,128)(2,1)S(1)}, u32[]{:S(2)}, u32[]{:S(2)}) async-start(bf16[4,96,256]{2,1,0:T(8,128)(2,1)} %copy.51), calls=%async_computation | async-start | bytes 393216 | tf_op jit(solution)/shard_map/all_to_all | solution.py:165
  187.3 4.3 %all-to-all-done = bf16[4,96,256]{2,1,0:T(8,128)(2,1)S(1)} async-done(((bf16[4,96,256]{2,1,0:T(8,128)(2,1)}), bf16[4,96,256]{2,1,0:T(8,128)(2,1)S(1)}, u32[]{:S(2)}, u32[]{:S(2)}) %all-to-all-start) | async-done | bytes 196640 | tf_op jit(solution)/shard_map/all_to_all | solution.py:165
  191.7 3.0 %convolution_convert_fusion.2 = bf16[96,2048]{1,0:T(8,128)(2,1)S(1)} fusion(bf16[96,1024]{1,0:T(8,128)(2,1)S(1)} %bitcast.139, bf16[1024,2048]{1,0:T(8,128)(2,1)} %all-gather.8.cloned.1.call-done), kind=kOutput, calls=%fused_computation.45 | convolution fusion | flops 402849792 | bytes 4784128 | tf_op jit(solution)/shard_map/dot_general | solution.py:172
  195.5 3.5 %all-to-all-start.1 = ((bf16[96,4,512]{2,0,1:T(8,128)(2,1)}), bf16[96,4,512]{2,0,1:T(8,128)(2,1)S(1)}, u32[]{:S(2)}, u32[]{:S(2)}) async-start(bf16[96,4,512]{2,0,1:T(8,128)(2,1)} %bitcast.109), calls=%async_computation.1 | async-start | bytes 786432 | tf_op jit(solution)/shard_map/all_to_all | solution.py:175
  199.0 3.0 %convolution_convert_fusion.1 = bf16[96,2048]{1,0:T(8,128)(2,1)S(1)} fusion(bf16[96,1024]{1,0:T(8,128)(2,1)S(1)} %bitcast.138, bf16[1024,2048]{1,0:T(8,128)(2,1)} %all-gather.10.cloned.1.call-done), kind=kOutput, calls=%fused_computation.44 | convolution fusion | flops 402849792 | bytes 4784128 | tf_op jit(solution)/shard_map/dot_general | solution.py:173
  202.8 3.6 %all-to-all-done.1 = bf16[96,4,512]{2,0,1:T(8,128)(2,1)S(1)} async-done(((bf16[96,4,512]{2,0,1:T(8,128)(2,1)}), bf16[96,4,512]{2,0,1:T(8,128)(2,1)S(1)}, u32[]{:S(2)}, u32[]{:S(2)}) %all-to-all-start.1) | async-done | bytes 393248 | tf_op jit(solution)/shard_map/all_to_all | solution.py:175
  206.3 3.5 %all-to-all-start.3 = ((bf16[96,4,512]{2,0,1:T(8,128)(2,1)}), bf16[96,4,512]{2,0,1:T(8,128)(2,1)S(1)}, u32[]{:S(2)}, u32[]{:S(2)}) async-start(bf16[96,4,512]{2,0,1:T(8,128)(2,1)} %bitcast.108), calls=%async_computation.3 | async-start | bytes 786432 | tf_op jit(solution)/shard_map/all_to_all | solution.py:178
  209.9 4.1 %fusion.26 = f32[384,512]{1,0:T(8,128)} fusion(f32[384,512]{1,0:T(8,128)S(1)} %bitcast.141, bf16[384,2048]{0,1:T(8,128)(2,1)} %copy-done.2, bf16[2048,512]{1,0:T(8,128)(2,1)} %param.36), kind=kOutput, calls=%fused_computation.52 | convolution fusion | flops 806092800 | bytes 5242880 | tf_op jit(solution)/shard_map/dot_general | solution.py:162
  214.0 3.2 %all-to-all-done.3 = bf16[96,4,512]{2,0,1:T(8,128)(2,1)S(1)} async-done(((bf16[96,4,512]{2,0,1:T(8,128)(2,1)}), bf16[96,4,512]{2,0,1:T(8,128)(2,1)S(1)}, u32[]{:S(2)}, u32[]{:S(2)}) %all-to-all-start.3) | async-done | bytes 393248 | tf_op jit(solution)/shard_map/all_to_all | solution.py:178
  217.3 4.1 %fusion.31 = bf16[384,512]{1,0:T(8,128)(2,1)} fusion(f32[384,512]{1,0:T(8,128)} %fusion.26, f32[384,512]{1,0:T(8,128)S(1)} %bitcast.140, bf16[384,2048]{0,1:T(8,128)(2,1)} %copy-done.2, bf16[2048,512]{1,0:T(8,128)(2,1)} %param.37), kind=kOutput, calls=%fused_computation.57 | convolution fusion | flops 806486016 | bytes 5636096 | tf_op jit(solution)/shard_map/dot_general | solution.py:163
  (294 shorter events, 68.9 us)
Async XLA Ops:
  6.5 46.6 %copy-start = (bf16[2048,512]{1,0:T(8,128)(2,1)S(1)}, bf16[2048,512]{1,0:T(8,128)(2,1)}, u32[]{:S(2)}) copy-start(bf16[2048,512]{1,0:T(8,128)(2,1)} %param.22) | copy-start | bytes 6291460
  6.5 24.7 %all-gather.12.cloned.1.call-start = ((), (), s32[]{:S(2)}) async-start(), calls=%async_computation.7 | async-start | bytes 1966080 | tf_op jit(solution)/shard_map/all_gather | solution.py:80
  7.3 89.5 %all-gather.6.cloned.1.call-start = ((), (), s32[]{:S(2)}) async-start(), calls=%async_computation.4 | async-start | bytes 1769472 | tf_op jit(solution)/shard_map/all_gather | solution.py:97
  31.3 3.6 %copy-start.6 = (bf16[1536,512]{1,0:T(8,128)(2,1)S(1)}, bf16[1536,512]{1,0:T(8,128)(2,1)}, u32[]{:S(2)}) copy-start(bf16[1536,512]{1,0:T(8,128)(2,1)} %all-gather.12.cloned.1.call-done) | copy-start | bytes 4718596
  35.3 3.6 %copy-start.12 = (f32[2048]{0:T(1024)S(1)}, f32[2048]{0:T(1024)}, u32[]{:S(2)}) copy-start(f32[2048]{0:T(1024)} %param.21) | copy-start | bytes 24580
  42.4 3.8 %copy-start.7 = (bf16[2048,256]{1,0:T(8,128)(2,1)S(1)}, bf16[2048,256]{1,0:T(8,128)(2,1)}, u32[]{:S(2)}) copy-start(bf16[2048,256]{1,0:T(8,128)(2,1)} %param.31) | copy-start | bytes 3145732
  43.2 148.5 %all-gather.8.cloned.1.call-start = ((), (), s32[]{:S(2)}) async-start(), calls=%async_computation.5 | async-start | bytes 5242880 | tf_op jit(solution)/shard_map/all_gather | solution.py:169
  44.0 155.0 %all-gather.10.cloned.1.call-start = ((), (), s32[]{:S(2)}) async-start(), calls=%async_computation.6 | async-start | bytes 5242880 | tf_op jit(solution)/shard_map/all_gather | solution.py:170
  45.2 7.9 %copy-start.3 = (bf16[384,2048]{0,1:T(8,128)(2,1)S(1)}, bf16[384,2048]{0,1:T(8,128)(2,1)}, u32[]{:S(2)}) copy-start(bf16[384,2048]{0,1:T(8,128)(2,1)} %copy-done.2) | copy-start | bytes 4718596
  48.3 42.2 %collective-permute-start = (bf16[8,256]{1,0:T(8,128)(2,1)S(1)}, bf16[8,256]{1,0:T(8,128)(2,1)S(1)}, u32[]{:S(2)}, u32[]{:S(2)}) collective-permute-start(bf16[8,256]{1,0:T(8,128)(2,1)S(1)} %get-tuple-element.163), channel_id=1, source_target_pairs={{0,4},{4,8},{8,12},{12,16},{16,20},{20,24},{24,28},{1,5},{5,9},{9,... | collective-permute-start | bytes 12296 | tf_op jit(solution)/shard_map/ppermute | solution.py:23
  51.7 2.6 %copy-start.8 = (bf16[512,384]{1,0:T(8,128)(2,1)S(1)}, bf16[512,384]{1,0:T(8,128)(2,1)}, u32[]{:S(2)}) copy-start(bf16[512,384]{1,0:T(8,128)(2,1)} %param.24) | copy-start | bytes 1179652
  51.7 2.6 %copy-start.13 = (f32[512]{0:T(512)S(1)}, f32[512]{0:T(512)}, u32[]{:S(2)}) copy-start(f32[512]{0:T(512)} %param.23) | copy-start | bytes 6148
  51.7 3.2 %copy-start.16 = (f32[96]{0:T(128)S(1)}, f32[96]{0:T(128)}, u32[]{:S(2)}) copy-start(f32[96]{0:T(128)} %param.29) | copy-start | bytes 1156
  51.7 38.8 %collective-permute-start.1 = (bf16[8,256]{1,0:T(8,128)(2,1)S(1)}, bf16[8,256]{1,0:T(8,128)(2,1)S(1)}, u32[]{:S(2)}, u32[]{:S(2)}) collective-permute-start(bf16[8,256]{1,0:T(8,128)(2,1)S(1)} %get-tuple-element.164), channel_id=1, source_target_pairs={{4,0},{8,4},{12,8},{16,12},{20,16},{24,20},{28,24},{5,1},{9,5},{13... | collective-permute-start | bytes 12296 | tf_op jit(solution)/shard_map/ppermute | solution.py:25
  55.2 35.4 %copy-start.18 = (bf16[1,256,256]{2,1,0:T(8,128)(2,1)S(1)}, bf16[1,256,256]{2,1,0:T(8,128)(2,1)}, u32[]{:S(2)}) copy-start(bf16[1,256,256]{2,1,0:T(8,128)(2,1)} %param.32) | copy-start | bytes 393220
  92.0 8.1 %copy-start.5 = (bf16[256,512]{1,0:T(8,128)(2,1)S(1)}, bf16[256,512]{1,0:T(8,128)(2,1)}, u32[]{:S(2)}) copy-start(bf16[256,512]{1,0:T(8,128)(2,1)} %param.28) | copy-start | bytes 786436
  92.7 90.3 %all-to-all-start.2 = ((bf16[4,96,256]{2,1,0:T(8,128)(2,1)}), bf16[4,96,256]{2,1,0:T(8,128)(2,1)}, u32[]{:S(2)}, u32[]{:S(2)}) async-start(bf16[4,96,256]{2,1,0:T(8,128)(2,1)} %multiply_convert_fusion.2), calls=%async_computation.2 | async-start | bytes 393216 | tf_op jit(solution)/shard_map/all_to_all | solution.py:166
  101.4 3.8 %copy-start.4 = (bf16[384,4,96]{0,2,1:T(8,128)(2,1)S(1)}, bf16[384,4,96]{0,2,1:T(8,128)(2,1)}, u32[]{:S(2)}) copy-start(bf16[384,4,96]{0,2,1:T(8,128)(2,1)} %get-tuple-element.283) | copy-start | bytes 884740 | tf_op jit(solution)/shard_map/while
  107.2 2.4 %copy-start.1 = (f32[4,384,384]{2,1,0:T(8,128)S(1)}, f32[4,384,384]{2,1,0:T(8,128)}, u32[]{:S(2)}) copy-start(f32[4,384,384]{2,1,0:T(8,128)} %get-tuple-element.245) | copy-start | bytes 7077892 | tf_op jit(solution)/shard_map/while
  111.6 3.8 %copy-start.4 = (bf16[384,4,96]{0,2,1:T(8,128)(2,1)S(1)}, bf16[384,4,96]{0,2,1:T(8,128)(2,1)}, u32[]{:S(2)}) copy-start(bf16[384,4,96]{0,2,1:T(8,128)(2,1)} %get-tuple-element.283) | copy-start | bytes 884740 | tf_op jit(solution)/shard_map/while
  117.4 2.4 %copy-start.1 = (f32[4,384,384]{2,1,0:T(8,128)S(1)}, f32[4,384,384]{2,1,0:T(8,128)}, u32[]{:S(2)}) copy-start(f32[4,384,384]{2,1,0:T(8,128)} %get-tuple-element.245) | copy-start | bytes 7077892 | tf_op jit(solution)/shard_map/while
  121.8 3.8 %copy-start.4 = (bf16[384,4,96]{0,2,1:T(8,128)(2,1)S(1)}, bf16[384,4,96]{0,2,1:T(8,128)(2,1)}, u32[]{:S(2)}) copy-start(bf16[384,4,96]{0,2,1:T(8,128)(2,1)} %get-tuple-element.283) | copy-start | bytes 884740 | tf_op jit(solution)/shard_map/while
  131.9 3.8 %copy-start.4 = (bf16[384,4,96]{0,2,1:T(8,128)(2,1)S(1)}, bf16[384,4,96]{0,2,1:T(8,128)(2,1)}, u32[]{:S(2)}) copy-start(bf16[384,4,96]{0,2,1:T(8,128)(2,1)} %get-tuple-element.283) | copy-start | bytes 884740 | tf_op jit(solution)/shard_map/while
  142.1 3.8 %copy-start.4 = (bf16[384,4,96]{0,2,1:T(8,128)(2,1)S(1)}, bf16[384,4,96]{0,2,1:T(8,128)(2,1)}, u32[]{:S(2)}) copy-start(bf16[384,4,96]{0,2,1:T(8,128)(2,1)} %get-tuple-element.283) | copy-start | bytes 884740 | tf_op jit(solution)/shard_map/while
  147.8 2.4 %copy-start.1 = (f32[4,384,384]{2,1,0:T(8,128)S(1)}, f32[4,384,384]{2,1,0:T(8,128)}, u32[]{:S(2)}) copy-start(f32[4,384,384]{2,1,0:T(8,128)} %get-tuple-element.245) | copy-start | bytes 7077892 | tf_op jit(solution)/shard_map/while
  152.3 3.8 %copy-start.4 = (bf16[384,4,96]{0,2,1:T(8,128)(2,1)S(1)}, bf16[384,4,96]{0,2,1:T(8,128)(2,1)}, u32[]{:S(2)}) copy-start(bf16[384,4,96]{0,2,1:T(8,128)(2,1)} %get-tuple-element.283) | copy-start | bytes 884740 | tf_op jit(solution)/shard_map/while
  162.4 3.8 %copy-start.4 = (bf16[384,4,96]{0,2,1:T(8,128)(2,1)S(1)}, bf16[384,4,96]{0,2,1:T(8,128)(2,1)}, u32[]{:S(2)}) copy-start(bf16[384,4,96]{0,2,1:T(8,128)(2,1)} %get-tuple-element.283) | copy-start | bytes 884740 | tf_op jit(solution)/shard_map/while
  172.5 3.8 %copy-start.4 = (bf16[384,4,96]{0,2,1:T(8,128)(2,1)S(1)}, bf16[384,4,96]{0,2,1:T(8,128)(2,1)}, u32[]{:S(2)}) copy-start(bf16[384,4,96]{0,2,1:T(8,128)(2,1)} %get-tuple-element.283) | copy-start | bytes 884740 | tf_op jit(solution)/shard_map/while
  178.3 2.4 %copy-start.1 = (f32[4,384,384]{2,1,0:T(8,128)S(1)}, f32[4,384,384]{2,1,0:T(8,128)}, u32[]{:S(2)}) copy-start(f32[4,384,384]{2,1,0:T(8,128)} %get-tuple-element.245) | copy-start | bytes 7077892 | tf_op jit(solution)/shard_map/while
  183.0 8.6 %all-to-all-start = ((bf16[4,96,256]{2,1,0:T(8,128)(2,1)}), bf16[4,96,256]{2,1,0:T(8,128)(2,1)S(1)}, u32[]{:S(2)}, u32[]{:S(2)}) async-start(bf16[4,96,256]{2,1,0:T(8,128)(2,1)} %copy.51), calls=%async_computation | async-start | bytes 393216 | tf_op jit(solution)/shard_map/all_to_all | solution.py:165
  195.5 10.8 %all-to-all-start.1 = ((bf16[96,4,512]{2,0,1:T(8,128)(2,1)}), bf16[96,4,512]{2,0,1:T(8,128)(2,1)S(1)}, u32[]{:S(2)}, u32[]{:S(2)}) async-start(bf16[96,4,512]{2,0,1:T(8,128)(2,1)} %bitcast.109), calls=%async_computation.1 | async-start | bytes 786432 | tf_op jit(solution)/shard_map/all_to_all | solution.py:175
  206.3 10.8 %all-to-all-start.3 = ((bf16[96,4,512]{2,0,1:T(8,128)(2,1)}), bf16[96,4,512]{2,0,1:T(8,128)(2,1)S(1)}, u32[]{:S(2)}, u32[]{:S(2)}) async-start(bf16[96,4,512]{2,0,1:T(8,128)(2,1)} %bitcast.108), calls=%async_computation.3 | async-start | bytes 786432 | tf_op jit(solution)/shard_map/all_to_all | solution.py:178
  (25 other events, 40.0 us)
Sparse Core Ops, SparseCore 0:
  8.9 22.3 all-gather.11
  43.4 46.0 all-gather.5
  91.0 35.0 all-gather.7
  127.5 33.5 all-gather.9
